TPU v7x, 32 devices: a whole 2x2x4 slice. The times are simulated.
32 devices in a mesh: sp: 4 (over z), dp: 8 (over y, x, core).
Axes of the slice: x: 2, y: 2, z: 4, core: 2. Of those that a mesh axis runs over, the one named last changes fastest.
Arguments:
- probe_vectors: bfloat16 [4096, 1024], P(('dp', 'sp')), may hold values from -6 to 6
- address_vectors: bfloat16 [4096, 1024], P(('dp', 'sp')), may hold values from -6 to 6
- content_vectors: bfloat16 [4096, 2048], P(('dp', 'sp')), may hold values from -6 to 6
- adjoint_of_result: bfloat16 [4096, 2048], P(('dp', 'sp')), may hold values from -0.5 to 0.5
- compact_factor: bfloat16 [4096, 64], P(('dp', 'sp')), may hold values from -7.5 to 7.5
- latent_to_damping_map: bfloat16 [64, 1024], replicated, may hold values from -0.75 to 0.75
- damping_shift_term: float32 [1024], replicated
- surplus_damping: bfloat16 [4096, 16], P(('dp', 'sp')), may hold values from -0.7 to 0
Outputs:
- query_grad: bfloat16 [4096, 1024], P(('dp', 'sp'))
- key_grad: bfloat16 [4096, 1024], P(('dp', 'sp'))
- value_grad: bfloat16 [4096, 2048], P(('dp', 'sp'))
- latent_grad: bfloat16 [4096, 64], P(('dp', 'sp'))
- weight_grad: float32 [64, 1024], replicated
All inputs are finite; a program needn't handle non-finite values.
Results may differ from a plain program's by a relative error of at most 0.005.
Values may be sent and summed in bfloat16 or wider, within the bound.
No kernel may reach another device: no remote copies, remote signals or barrier semaphores. Data moves between devices by JAX's collectives and lax.ppermute only.
A program may use at most 64 MiB of HBM per device.

v0:
```python
import jax
import jax.numpy as jnp
from jax import lax
from jax.sharding import PartitionSpec as P

KEY_CHANNELS = 64
VALUE_DIM = 128
BLOCK = 64
gate_norm = 16.0
highest = lax.Precision.HIGHEST


def carry_states(block_total, increments):
    log_totals = block_total[:, :, 0, :]
    running = jnp.cumsum(log_totals, axis=1)
    before = running - log_totals
    blocks = log_totals.shape[1]
    order = jnp.arange(blocks, dtype=jnp.int32)
    earlier_mask = (order[None, :] < order[:, None])[None, :, :, None]
    exponent = before[:, :, None, :] - running[:, None, :, :]
    exponent = jnp.where(earlier_mask, exponent, jnp.zeros_like(exponent))
    weights = jnp.where(earlier_mask, jnp.exp(exponent), jnp.zeros_like(exponent))
    return jnp.einsum("hnmk,mhkv->nhkv", weights, increments, precision=highest)


def gla_forward(probe_vectors, address_vectors, content_vectors, logarithm_decay):
    head_count, seq_len, key_width = probe_vectors.shape
    value_width = content_vectors.shape[2]
    blocks = seq_len // BLOCK

    def blocked(tensor):
        return tensor.reshape(head_count, blocks, BLOCK, tensor.shape[2])

    cumulative = jnp.cumsum(blocked(logarithm_decay), axis=2)
    block_total = cumulative[:, :, BLOCK - 1 :, :]
    keys_block = blocked(address_vectors)
    query_decayed = blocked(probe_vectors) * key_width ** (-0.5) * jnp.exp(cumulative)
    key_inverse = keys_block * jnp.exp(-cumulative)
    key_to_end = keys_block * jnp.exp(block_total - cumulative)
    value_block = blocked(content_vectors)
    scores = jnp.einsum("hnik,hnjk->hnij", query_decayed, key_inverse, precision=highest)
    positions = jnp.arange(BLOCK, dtype=jnp.int32)
    causal = positions[:, None] >= positions[None, :]
    scores = jnp.where(causal, scores, jnp.zeros_like(scores))
    within_block = jnp.einsum("hnij,hnjv->hniv", scores, value_block, precision=highest)
    increments = jnp.einsum("hnjk,hnjv->nhkv", key_to_end, value_block, precision=highest)
    earlier = carry_states(block_total, increments)
    carried = jnp.einsum("hnik,nhkv->hniv", query_decayed, earlier, precision=highest)
    return (within_block + carried).reshape(head_count, seq_len, value_width)


def split_into_heads(tensor, width):
    return tensor.astype(jnp.float32).reshape(tensor.shape[0], -1, width).transpose(1, 0, 2)


def to_rows(tensor):
    return tensor.transpose(1, 0, 2).reshape(tensor.shape[1], tensor.shape[0] * tensor.shape[2])


def on_device(
    probe_vectors,
    address_vectors,
    content_vectors,
    adjoint_of_result,
    compact_factor,
    latent_to_damping_map,
    damping_shift_term,
    surplus_damping,
):
    query_per_head, key_per_head, value_per_head, upstream_heads, spike_heads = (
        lax.all_to_all(probe_vectors, "sp", split_axis=1, concat_axis=0, tiled=True),
        lax.all_to_all(address_vectors, "sp", split_axis=1, concat_axis=0, tiled=True),
        lax.all_to_all(content_vectors, "sp", split_axis=1, concat_axis=0, tiled=True),
        lax.all_to_all(adjoint_of_result, "sp", split_axis=1, concat_axis=0, tiled=True),
        lax.all_to_all(surplus_damping, "sp", split_axis=1, concat_axis=0, tiled=True),
    )
    local_width = query_per_head.shape[1]
    hidden_code_rows = lax.all_gather(compact_factor, "sp", axis=0, tiled=True)
    column_start = lax.axis_index("sp") * local_width
    weight_local = lax.dynamic_slice_in_dim(latent_to_damping_map, column_start, local_width, 1)
    bias_local = lax.dynamic_slice_in_dim(damping_shift_term, column_start, local_width, 0)
    gate_logit = (
        jnp.dot(hidden_code_rows, weight_local, preferred_element_type=jnp.float32) + bias_local
    )
    forget_rate_rows = jax.nn.log_sigmoid(gate_logit) / gate_norm
    logarithm_decay = (
        split_into_heads(forget_rate_rows, KEY_CHANNELS)
        + spike_heads.astype(jnp.float32).T[:, :, None]
    )
    _, pullback = jax.vjp(
        gla_forward,
        split_into_heads(query_per_head, KEY_CHANNELS),
        split_into_heads(key_per_head, KEY_CHANNELS),
        split_into_heads(value_per_head, VALUE_DIM),
        logarithm_decay,
    )
    grad_query, grad_key, grad_value, grad_decay = pullback(
        split_into_heads(upstream_heads, VALUE_DIM)
    )
    query_grad, key_grad, value_grad = (
        lax.all_to_all(
            to_rows(grad_query).astype(jnp.bfloat16), "sp", split_axis=0, concat_axis=1, tiled=True
        ),
        lax.all_to_all(
            to_rows(grad_key).astype(jnp.bfloat16), "sp", split_axis=0, concat_axis=1, tiled=True
        ),
        lax.all_to_all(
            to_rows(grad_value).astype(jnp.bfloat16), "sp", split_axis=0, concat_axis=1, tiled=True
        ),
    )
    decay_rows = to_rows(grad_decay)
    gate_grad = (decay_rows * jax.nn.sigmoid(-gate_logit) / gate_norm).astype(jnp.bfloat16)
    partial_latent = jnp.einsum(
        "sc,rc->sr", gate_grad, weight_local, preferred_element_type=jnp.float32
    )
    latent_grad = lax.psum_scatter(partial_latent, "sp", scatter_dimension=0, tiled=True).astype(
        jnp.bfloat16
    )
    local_weight = jnp.einsum(
        "sr,sc->rc", hidden_code_rows, gate_grad, preferred_element_type=jnp.float32
    )
    summed = lax.psum(local_weight, "dp")
    weight_grad = lax.all_gather(summed, "sp", axis=1, tiled=True)
    return (query_grad, key_grad, value_grad, latent_grad, weight_grad)


def solution(mesh):
    return jax.shard_map(
        on_device,
        mesh=mesh,
        in_specs=(
            P(("dp", "sp"), None),
            P(("dp", "sp"), None),
            P(("dp", "sp"), None),
            P(("dp", "sp"), None),
            P(("dp", "sp"), None),
            P(),
            P(),
            P(("dp", "sp"), None),
        ),
        out_specs=(
            P(("dp", "sp"), None),
            P(("dp", "sp"), None),
            P(("dp", "sp"), None),
            P(("dp", "sp"), None),
            P(),
        ),
        check_vma=False,
    )
```

profile of v0, /device:TPU:0, one launch (start us, length us, event | category | flops | bytes accessed | tf_op | source)
XLA Modules:
  0.0 277.0 jit_solution(3052615414394250195)
XLA Ops:
  8.0 6.5 %all-to-all-start.1 = ((bf16[128,4,4]{0,2,1:T(4,128)(2,1)}), bf16[128,4,4]{0,2,1:T(4,128)(2,1)S(1)}, u32[]{:S(2)}, u32[]{:S(2)}) async-start(bf16[128,4,4]{0,2,1:T(4,128)(2,1)} %bitcast.169), calls=%async_computation.1 | async-start | bytes 8192 | tf_op jit(solution)/shard_map/all_to_all | solution.py:75
  14.5 1.8 copy.214
  16.3 3.8 %all-to-all-done.1 = bf16[128,4,4]{0,2,1:T(4,128)(2,1)S(1)} async-done(((bf16[128,4,4]{0,2,1:T(4,128)(2,1)}), bf16[128,4,4]{0,2,1:T(4,128)(2,1)S(1)}, u32[]{:S(2)}, u32[]{:S(2)}) %all-to-all-start.1) | async-done | bytes 4128 | tf_op jit(solution)/shard_map/all_to_all | solution.py:75
  20.1 3.5 %all-to-all-start.5 = ((bf16[128,4,256]{0,2,1:T(8,128)(2,1)}), bf16[128,4,256]{0,2,1:T(8,128)(2,1)S(1)}, u32[]{:S(2)}, u32[]{:S(2)}) async-start(bf16[128,4,256]{0,2,1:T(8,128)(2,1)} %bitcast.24), calls=%async_computation.5 | async-start | bytes 524288 | tf_op jit(solution)/shard_map/all_to_all | solution.py:71
  24.5 7.0 %all-to-all-done.5 = bf16[128,4,256]{0,2,1:T(8,128)(2,1)S(1)} async-done(((bf16[128,4,256]{0,2,1:T(8,128)(2,1)}), bf16[128,4,256]{0,2,1:T(8,128)(2,1)S(1)}, u32[]{:S(2)}, u32[]{:S(2)}) %all-to-all-start.5) | async-done | bytes 262176 | tf_op jit(solution)/shard_map/all_to_all | solution.py:71
  31.5 3.4 %all-to-all-start = ((bf16[128,4,256]{0,2,1:T(8,128)(2,1)}), bf16[128,4,256]{0,2,1:T(8,128)(2,1)S(1)}, u32[]{:S(2)}, u32[]{:S(2)}) async-start(bf16[128,4,256]{0,2,1:T(8,128)(2,1)} %bitcast), calls=%async_computation | async-start | bytes 524288 | tf_op jit(solution)/shard_map/all_to_all | solution.py:72
  36.6 12.5 %all_gather.6 = bf16[512,64]{0,1:T(8,128)(2,1)S(1)} all-gather(bf16[128,64]{0,1:T(8,128)(2,1)S(1)} %copy-done.31), channel_id=1, replica_groups=mesh['sp'=4,'dp'=8] {'sp'}, dimensions={0}, use_global_device_ids=true | all-gather | bytes 81920 | tf_op jit(solution)/shard_map/all_gather | solution.py:78
  51.7 4.1 %all-to-all-start.3 = ((bf16[128,4,512]{2,0,1:T(8,128)(2,1)}), bf16[128,4,512]{2,0,1:T(8,128)(2,1)}, u32[]{:S(2)}, u32[]{:S(2)}) async-start(bf16[128,4,512]{2,0,1:T(8,128)(2,1)} %bitcast.143), calls=%async_computation.3 | async-start | bytes 1048576 | tf_op jit(solution)/shard_map/all_to_all | solution.py:74
  58.0 25.9 %fusion.46 = f32[4,8,64,64]{3,1,2,0:T(8,128)S(1)} fusion(f32[4,8,64,64]{3,1,2,0:T(8,128)S(1)} %copy.194), kind=kOutput, calls=%fused_computation.84 | output fusion | flops 8257536 | bytes 1048576 | tf_op jit(solution)/shard_map/jvp(jit(cumsum))/reduce_window_sum | solution.py:34
  83.9 5.1 %all-to-all-start.2 = ((bf16[128,4,512]{2,0,1:T(8,128)(2,1)}), bf16[128,4,512]{2,0,1:T(8,128)(2,1)}, u32[]{:S(2)}, u32[]{:S(2)}) async-start(bf16[128,4,512]{2,0,1:T(8,128)(2,1)} %bitcast.144), calls=%async_computation.2 | async-start | bytes 1048576 | tf_op jit(solution)/shard_map/all_to_all | solution.py:73
  95.1 2.0 reshape.161
  97.0 1.9 copy.205
  99.4 2.0 reshape.159
  103.7 2.9 %convolution_bitcast_fusion = f32[8,4,64,128]{3,0,2,1:T(8,128)S(1)} fusion(f32[4,64,128,8]{2,1,3,0:T(8,128)S(1)} %convolution_bitcast_fusion.3, f32[4,8,64]{1,2,0:T(8,128)S(1)} %copy-done.23, f32[4,8,64]{1,2,0:T(8,128)S(1)} %copy-done.24, pred[8,8]{1,0:T(8,128)(4,1)S(1)} %copy-done.32), kind=kOutput, calls=%fused_computation.4 | convolution fusion | flops 25214976 | bytes 2113600 | tf_op jit(solution)/shard_map/transpose(jvp(hnmk,mhkv->nhkv))/dot_general | solution.py:23
  106.6 2.8 %fusion.18 = (f32[4,8,64]{2,1,0:T(8,128)}, f32[4,8,64,64]{2,3,1,0:T(8,128)S(1)}, f32[4,8,64,64]{2,3,1,0:T(8,128)}) fusion(f32[4,8,64,64]{2,3,1,0:T(8,128)S(1)} %copy.195, f32[4,8,64,64]{2,1,3,0:T(8,128)S(1)} %reshape.166, f32[4,8,64]{2,1,0:T(8,128)S(1)} %slice_bitcast_fusion, bf16[4,8,64,128]{3,2,1,0:T(8,128)(2,1)S(1)} %bitcast.150, ...), kind=kOutput, calls=%fused_computation.40 | convolution fusion | flops 201979904 | bytes 3686400 | tf_op jit(solution)/shard_map/transpose(jvp(hnjk,hnjv->nhkv))/dot_general | solution.py:46
  110.4 2.5 convolution_bitcast_fusion.1
  112.9 4.3 %fusion.45 = (f32[4,8,64]{1,2,0:T(8,128)}, f32[4,8,64]{1,2,0:T(8,128)}) fusion(f32[4,8,64]{1,2,0:T(8,128)S(1)} %copy-done.23, f32[4,8,64]{1,2,0:T(8,128)S(1)} %copy-done.24, f32[8,4,64,128]{3,2,1,0:T(8,128)S(1)} %fusion.6, f32[4,64,128,8]{2,1,3,0:T(8,128)S(1)} %convolution_bitcast_fusion.3, pred[8,8]{1,0:T(8,128)(4,1)S(1)} %copy-done.32), kind=kOutput, calls=%fused_computation.83 | convolution fusion | flops 25276416 | bytes 2129984 | tf_op jit(solution)/shard_map/transpose(jvp(hnmk,mhkv->nhkv))/dot_general | solution.py:23
  117.3 2.0 convolution_bitcast_fusion.4
  122.2 1.4 copy.244
  123.6 1.4 copy.245
  125.1 1.6 convolution_select_fusion
  128.6 1.5 fusion.3
  130.1 3.7 %pad_add_fusion = (f32[4,8,64,64]{2,3,1,0:T(8,128)}, bf16[4,8,64,64]{2,3,1,0:T(8,128)(2,1)}, bf16[4,8,64,64]{2,3,1,0:T(8,128)(2,1)S(1)}) fusion(f32[4,8,1,64]{2,3,1,0:T(8,128)S(1)} %fusion.3, f32[4,8,64,64]{2,3,1,0:T(8,128)S(1)} %fusion.44, f32[4,8,64,64]{2,1,3,0:T(8,128)S(1)} %mul.72, f32[4,8,64,64]{2,3,1,0:T(8,128)S(1)} %copy.195, ...), kind=kOutput, calls=%fused_computation.22 | convolution fusion | flops 103677952 | bytes 4734976 | tf_op jit(solution)/shard_map/transpose(jvp(hnik,hnjk->hnij))/dot_general | solution.py:41
  137.1 1.7 copy.213
  138.8 4.8 %all-to-all-start.4 = ((bf16[4,128,256]{1,2,0:T(8,128)(2,1)}), bf16[4,128,256]{1,2,0:T(8,128)(2,1)S(1)}, u32[]{:S(2)}, u32[]{:S(2)}) async-start(bf16[4,128,256]{1,2,0:T(8,128)(2,1)} %copy.213), calls=%async_computation.4 | async-start | bytes 524288 | tf_op jit(solution)/shard_map/all_to_all | solution.py:101
  143.6 3.1 %convolution_select_fusion.2 = f32[4,8,64,64]{3,2,1,0:T(8,128)} fusion(pred[64,64]{1,0:T(8,128)(4,1)S(1)} %copy-done.28, f32[4,8,64,64]{2,1,3,0:T(8,128)S(1)} %reshape.166, f32[4,8,64,64]{2,3,1,0:T(8,128)S(1)} %copy.195, f32[4,8,64,64]{2,1,3,0:T(8,128)S(1)} %mul.72), kind=kOutput, calls=%fused_computation.11 | convolution fusion | flops 101187584 | bytes 2101248 | tf_op jit(solution)/shard_map/jvp(hnik,hnjk->hnij)/dot_general | solution.py:41
  148.3 3.2 %fusion.11 = f32[4,8,64,128]{3,2,1,0:T(8,128)S(1)} fusion(f32[4,8,64,64]{2,3,1,0:T(8,128)S(1)} %copy-done.4, f32[8,4,64,128]{3,0,2,1:T(8,128)} %copy-done.9), kind=kOutput, calls=%fused_computation.30 | convolution fusion | flops 201326592 | bytes 2621440 | tf_op jit(solution)/shard_map/transpose(jvp(hnjk,hnjv->nhkv))/dot_general | solution.py:46
  151.5 5.2 %all-to-all-start.6 = ((bf16[4,128,256]{1,2,0:T(8,128)(2,1)}), bf16[4,128,256]{1,2,0:T(8,128)(2,1)S(1)}, u32[]{:S(2)}, u32[]{:S(2)}) async-start(bf16[4,128,256]{1,2,0:T(8,128)(2,1)} %copy.226), calls=%async_computation.6 | async-start | bytes 524288 | tf_op jit(solution)/shard_map/all_to_all | solution.py:104
  159.6 25.8 %fusion.47 = f32[4,8,64,64]{3,1,2,0:T(8,128)S(1)} fusion(f32[4,8,64,64]{3,1,2,0:T(8,128)S(1)} %copy.246), kind=kOutput, calls=%fused_computation.85 | output fusion | flops 8257536 | bytes 1048576 | tf_op jit(solution)/shard_map/transpose(jvp(jit(cumsum)))/reduce_window_sum | solution.py:34
  186.1 5.2 %all-to-all-start.7 = ((bf16[4,128,512]{2,1,0:T(8,128)(2,1)}), bf16[4,128,512]{2,1,0:T(8,128)(2,1)S(1)}, u32[]{:S(2)}, u32[]{:S(2)}) async-start(bf16[4,128,512]{2,1,0:T(8,128)(2,1)} %convert_element_type.84), calls=%async_computation.7 | async-start | bytes 1048576 | tf_op jit(solution)/shard_map/all_to_all | solution.py:107
  193.9 56.5 %all-reduce.3.cloned.1.call-done = f32[64,256]{1,0:T(8,128)} async-done(((f32[64,256]{1,0:T(8,128)}), f32[64,256]{1,0:T(8,128)}) %all-reduce.3.cloned.1.call-update) | async-done | bytes 65552 | tf_op jit(solution)/shard_map/psum | solution.py:122
  250.4 14.1 %all_gather.7 = f32[64,1024]{1,0:T(8,128)S(1)} all-gather(f32[64,256]{1,0:T(8,128)} %all-reduce.3.cloned.1.call-done), channel_id=1, replica_groups=mesh['sp'=4,'dp'=8] {'sp'}, dimensions={1}, use_global_device_ids=true | all-gather | bytes 327680 | tf_op jit(solution)/shard_map/all_gather | solution.py:123
  (132 shorter events, 37.8 us)
Async XLA Ops:
  8.0 41.7 %copy-start = (bf16[64,1024]{1,0:T(8,128)(2,1)S(1)}, bf16[64,1024]{1,0:T(8,128)(2,1)}, u32[]{:S(2)}) copy-start(bf16[64,1024]{1,0:T(8,128)(2,1)} %param.13) | copy-start | bytes 393220
  8.0 12.1 %all-to-all-start.1 = ((bf16[128,4,4]{0,2,1:T(4,128)(2,1)}), bf16[128,4,4]{0,2,1:T(4,128)(2,1)S(1)}, u32[]{:S(2)}, u32[]{:S(2)}) async-start(bf16[128,4,4]{0,2,1:T(4,128)(2,1)} %bitcast.169), calls=%async_computation.1 | async-start | bytes 8192 | tf_op jit(solution)/shard_map/all_to_all | solution.py:75
  20.1 3.6 %copy-start.20 = (bf16[128,1024]{1,0:T(8,128)(2,1)S(1)}, bf16[128,1024]{1,0:T(8,128)(2,1)}, u32[]{:S(2)}) copy-start(bf16[128,1024]{1,0:T(8,128)(2,1)} %param.9) | copy-start | bytes 786436
  20.1 11.4 %all-to-all-start.5 = ((bf16[128,4,256]{0,2,1:T(8,128)(2,1)}), bf16[128,4,256]{0,2,1:T(8,128)(2,1)S(1)}, u32[]{:S(2)}, u32[]{:S(2)}) async-start(bf16[128,4,256]{0,2,1:T(8,128)(2,1)} %bitcast.24), calls=%async_computation.5 | async-start | bytes 524288 | tf_op jit(solution)/shard_map/all_to_all | solution.py:71
  23.6 11.3 %copy-start.17 = (bf16[128,2048]{1,0:T(8,128)(2,1)S(1)}, bf16[128,2048]{1,0:T(8,128)(2,1)}, u32[]{:S(2)}) copy-start(bf16[128,2048]{1,0:T(8,128)(2,1)} %param.11) | copy-start | bytes 1572868
  31.5 19.5 %all-to-all-start = ((bf16[128,4,256]{0,2,1:T(8,128)(2,1)}), bf16[128,4,256]{0,2,1:T(8,128)(2,1)S(1)}, u32[]{:S(2)}, u32[]{:S(2)}) async-start(bf16[128,4,256]{0,2,1:T(8,128)(2,1)} %bitcast), calls=%async_computation | async-start | bytes 524288 | tf_op jit(solution)/shard_map/all_to_all | solution.py:72
  35.0 1.6 copy-start.31
  49.0 1.9 copy-start.21
  51.0 5.4 %copy-start.18 = (bf16[128,2048]{1,0:T(8,128)(2,1)S(1)}, bf16[128,2048]{1,0:T(8,128)(2,1)}, u32[]{:S(2)}) copy-start(bf16[128,2048]{1,0:T(8,128)(2,1)} %param.10) | copy-start | bytes 1572868
  51.7 32.2 %all-to-all-start.3 = ((bf16[128,4,512]{2,0,1:T(8,128)(2,1)}), bf16[128,4,512]{2,0,1:T(8,128)(2,1)}, u32[]{:S(2)}, u32[]{:S(2)}) async-start(bf16[128,4,512]{2,0,1:T(8,128)(2,1)} %bitcast.143), calls=%async_computation.3 | async-start | bytes 1048576 | tf_op jit(solution)/shard_map/all_to_all | solution.py:74
  83.9 15.5 %all-to-all-start.2 = ((bf16[128,4,512]{2,0,1:T(8,128)(2,1)}), bf16[128,4,512]{2,0,1:T(8,128)(2,1)}, u32[]{:S(2)}, u32[]{:S(2)}) async-start(bf16[128,4,512]{2,0,1:T(8,128)(2,1)} %bitcast.144), calls=%async_computation.2 | async-start | bytes 1048576 | tf_op jit(solution)/shard_map/all_to_all | solution.py:73
  102.5 7.0 %copy-start.5 = (bf16[4,512,128]{2,1,0:T(8,128)(2,1)}, bf16[4,512,128]{2,1,0:T(8,128)(2,1)S(1)}, u32[]{:S(2)}) copy-start(bf16[4,512,128]{2,1,0:T(8,128)(2,1)S(1)} %copy.198) | copy-start | bytes 1572868
  106.6 2.9 %copy-start.9 = (f32[8,4,64,128]{3,0,2,1:T(8,128)}, f32[8,4,64,128]{3,0,2,1:T(8,128)S(1)}, u32[]{:S(2)}) copy-start(f32[8,4,64,128]{3,0,2,1:T(8,128)S(1)} %convolution_bitcast_fusion) | copy-start | bytes 3145732
  117.3 2.0 copy-start.26
  122.2 1.4 copy-start.29
  123.6 1.4 copy-start.27
  126.7 1.3 copy-start.11
  126.7 1.5 copy-start.12
  126.7 1.8 copy-start.13
  128.5 1.5 copy-start.8
  128.5 1.5 copy-start.10
  138.8 4.8 %copy-start.28 = (pred[64,64]{1,0:T(8,128)(4,1)S(1)}, pred[64,64]{1,0:T(8,128)(4,1)}, u32[]{:S(2)}) copy-start(pred[64,64]{1,0:T(8,128)(4,1)} %iota_compare_fusion) | copy-start | bytes 12292
  138.8 12.7 %all-to-all-start.4 = ((bf16[4,128,256]{1,2,0:T(8,128)(2,1)}), bf16[4,128,256]{1,2,0:T(8,128)(2,1)S(1)}, u32[]{:S(2)}, u32[]{:S(2)}) async-start(bf16[4,128,256]{1,2,0:T(8,128)(2,1)} %copy.213), calls=%async_computation.4 | async-start | bytes 524288 | tf_op jit(solution)/shard_map/all_to_all | solution.py:101
  143.6 3.1 %copy-start.14 = (bf16[4,8,64,64]{2,3,1,0:T(8,128)(2,1)S(1)}, bf16[4,8,64,64]{2,3,1,0:T(8,128)(2,1)}, u32[]{:S(2)}) copy-start(bf16[4,8,64,64]{2,3,1,0:T(8,128)(2,1)} %get-tuple-element.23) | copy-start | bytes 786436
  148.3 8.4 %copy-start.6 = (f32[4,8,64,64]{3,2,1,0:T(8,128)S(1)}, f32[4,8,64,64]{3,2,1,0:T(8,128)}, u32[]{:S(2)}) copy-start(f32[4,8,64,64]{3,2,1,0:T(8,128)} %convolution_select_fusion.2) | copy-start | bytes 1572868
  151.5 5.3 %copy-start.2 = (bf16[4,512,128]{2,1,0:T(8,128)(2,1)S(1)}, bf16[4,512,128]{2,1,0:T(8,128)(2,1)}, u32[]{:S(2)}) copy-start(bf16[4,512,128]{2,1,0:T(8,128)(2,1)} %copy.205) | copy-start | bytes 1572868
  151.5 34.6 %all-to-all-start.6 = ((bf16[4,128,256]{1,2,0:T(8,128)(2,1)}), bf16[4,128,256]{1,2,0:T(8,128)(2,1)S(1)}, u32[]{:S(2)}, u32[]{:S(2)}) async-start(bf16[4,128,256]{1,2,0:T(8,128)(2,1)} %copy.226), calls=%async_computation.6 | async-start | bytes 524288 | tf_op jit(solution)/shard_map/all_to_all | solution.py:104
  157.7 1.4 copy-start.7
  186.1 5.3 %copy-start.19 = (f32[256,512]{1,0:T(8,128)S(1)}, f32[256,512]{1,0:T(8,128)}, u32[]{:S(2)}) copy-start(f32[256,512]{1,0:T(8,128)} %get-tuple-element.30) | copy-start | bytes 1572868
  186.1 81.5 %all-to-all-start.7 = ((bf16[4,128,512]{2,1,0:T(8,128)(2,1)}), bf16[4,128,512]{2,1,0:T(8,128)(2,1)S(1)}, u32[]{:S(2)}, u32[]{:S(2)}) async-start(bf16[4,128,512]{2,1,0:T(8,128)(2,1)} %convert_element_type.84), calls=%async_computation.7 | async-start | bytes 1048576 | tf_op jit(solution)/shard_map/all_to_all | solution.py:107
  191.3 59.1 %all-reduce.3.cloned.1.call-start = ((), (), s32[]{:S(2)}) async-start(), calls=%async_computation.10 | async-start | bytes 131072 | tf_op jit(solution)/shard_map/psum | solution.py:122
  193.0 71.5 %reduce-scatter.2.cloned.1.call-start = ((), (), s32[]{:S(2)}) async-start(), calls=%async_computation.9 | async-start | bytes 163840 | tf_op jit(solution)/shard_map/reduce_scatter | solution.py:116
  (11 other events, 10.9 us)
Sparse Core Ops, SparseCore 0:
  195.7 54.6 all-reduce.2
Sparse Core Ops, SparseCore 1:
  196.3 20.9 reduce-scatter.1
where the time goes:
time: 279 us; the launch traced here: 277 us
  waiting for transfers between devices  67.7 us (24%)
  other arithmetic  56 us (20%)
  local copies, waits for them, and re-layouts  39.8 us (14%)
  starting transfers between devices  38 us (14%)
  matrix products  32.9 us (12%)
  blocking collectives  26.6 us (10%)
  between operations  15.9 us (6%)
    psum x1, waiting for transfers between devices, on_device(): summed = lax.psum(local_weight, 'dp')  56.5 us
    another operation x2, other arithmetic, gla_forward(): cumulative = jnp.cumsum(blocked(logarithm_decay), axis=2)  51.6 us
    all_gather x1, blocking collectives, on_device(): weight_grad = lax.all_gather(summed, 'sp', axis=1, tiled=True)  14.1 us
    all_gather x1, blocking collectives, on_device(): hidden_code_rows = lax.all_gather(compact_factor, 'sp', axis=0, tiled=True)  12.5 us
    unnamed x72, local copies, waits for them, and re-layouts  10.3 us
    dot_general x3, matrix products, carry_states(): return jnp.einsum('hnmk,mhkv->nhkv', weights, increments, precision=highest)  9.75 us
    dot_general x3, matrix products, gla_forward(): jnp.einsum('hnik,hnjk->hnij', query_decayed, key_inverse, precision=highest)  8.12 us
    all_to_all x1, waiting for transfers between devices, on_device(): lax.all_to_all(probe_vectors, 'sp', split_axis=1, concat_axis=0, tiled=True)  7.02 us
  transfers between devices with their start and end apart: 10, of which 4 were waited for; matrix products, arithmetic and copies ran while one was open for 31% of the time, Pallas kernels for 0%

commit v1 on v0

--- a/solution.py
+++ b/solution.py
@@ -120,7 +120,12 @@
         "sr,sc->rc", hidden_code_rows, gate_grad, preferred_element_type=jnp.float32
     )
     summed = lax.psum(local_weight, "dp")
-    weight_grad = lax.all_gather(summed, "sp", axis=1, tiled=True)
+    ring = [summed]
+    for hop in range(3):
+        ring.append(lax.ppermute(ring[-1], "sp", [(dev, (dev + 1) % 4) for dev in range(4)]))
+    weight_grad = jnp.roll(
+        jnp.concatenate(ring[::-1], axis=1), (lax.axis_index("sp") + 1) * ring[0].shape[1], axis=1
+    )
     return (query_grad, key_grad, value_grad, latent_grad, weight_grad)
 
 

time: 279 us -> 256 us (0.918)
  other arithmetic: 56 us -> 34.7 us
  blocking collectives: 26.6 us -> 12.5 us
  local copies, waits for them, and re-layouts: 39.8 us -> 47 us
  waiting for transfers between devices: 67.7 us -> 74.1 us
    another operation x2, other arithmetic: 51.6 us -> 29.2 us  [gla_forward(): cumulative = jnp.cumsum(blocked(logarithm_decay), axis=2)]
    all_gather x1 -> x0, blocking collectives: 14.1 us -> none  [on_device(): weight_grad = lax.all_gather(summed, 'sp', axis=1, tiled=True)]
    psum x1, waiting for transfers between devices: 56.5 us -> 44.4 us  [on_device(): summed = lax.psum(local_weight, 'dp')]
    reduce_scatter x1, waiting for transfers between devices: 0.01 us -> 9.19 us  [on_device(): lax.psum_scatter(partial_latent, 'sp', scatter_dimension=0, tiled=True)]
    ppermute x0 -> x3, waiting for transfers between devices: none -> 5.63 us  [on_device(): lax.ppermute(ring[-1], 'sp', [(dev, (dev + 1) % 4) for dev in range(4)])]
    all_to_all x1, waiting for transfers between devices: 0.01 us -> 3.66 us  [on_device(): lax.all_to_all(to_rows(grad_key).astype(jnp.bfloat16), 'sp', split_axis=0...]
    unnamed x72 -> x78, local copies, waits for them, and re-layouts: 10.3 us -> 13.9 us
    convert_element_type x4, local copies, waits for them, and re-layouts: 4.98 us -> 1.47 us  [on_device(): to_rows(grad_query).astype(jnp.bfloat16)]
  transfers between devices with their start and end apart: 10 -> 13, of which waited for: 4 -> 8; matrix products, arithmetic and copies ran while one was open for 31% -> 25% of each run, Pallas kernels for 0% -> 0%
where the time goes in v1:
time: 256 us; the launch traced here: 255 us
  waiting for transfers between devices  74.1 us (29%)
  local copies, waits for them, and re-layouts  47 us (18%)
  starting transfers between devices  37.4 us (15%)
  other arithmetic  34.7 us (14%)
  matrix products  33 us (13%)
  between operations  16 us (6%)
  blocking collectives  12.5 us (5%)
    psum x1, waiting for transfers between devices, on_device(): summed = lax.psum(local_weight, 'dp')  44.4 us
    another operation x2, other arithmetic, gla_forward(): cumulative = jnp.cumsum(blocked(logarithm_decay), axis=2)  29.2 us
    unnamed x78, local copies, waits for them, and re-layouts  13.9 us
    all_gather x1, blocking collectives, on_device(): hidden_code_rows = lax.all_gather(compact_factor, 'sp', axis=0, tiled=True)  12.5 us
    dot_general x3, matrix products, carry_states(): return jnp.einsum('hnmk,mhkv->nhkv', weights, increments, precision=highest)  9.75 us
    reduce_scatter x1, waiting for transfers between devices, on_device(): lax.psum_scatter(partial_latent, 'sp', scatter_dimension=0, tiled=True)  9.19 us
    dot_general x3, matrix products, gla_forward(): jnp.einsum('hnik,hnjk->hnij', query_decayed, key_inverse, precision=highest)  8.21 us
    all_to_all x1, waiting for transfers between devices, on_device(): lax.all_to_all(probe_vectors, 'sp', split_axis=1, concat_axis=0, tiled=True)  7.02 us
  transfers between devices with their start and end apart: 13, of which 8 were waited for; matrix products, arithmetic and copies ran while one was open for 25% of the time, Pallas kernels for 0%

profile of v1, /device:TPU:0, one launch (start us, length us, event | category | flops | bytes accessed | tf_op | source)
XLA Modules:
  0.0 254.6 jit_solution(11525741730956779132)
XLA Ops:
  8.0 6.5 %all-to-all-start.1 = ((bf16[128,4,4]{0,2,1:T(4,128)(2,1)}), bf16[128,4,4]{0,2,1:T(4,128)(2,1)S(1)}, u32[]{:S(2)}, u32[]{:S(2)}) async-start(bf16[128,4,4]{0,2,1:T(4,128)(2,1)} %bitcast.168), calls=%async_computation.1 | async-start | bytes 8192 | tf_op jit(solution)/shard_map/all_to_all | solution.py:75
  16.3 3.8 %all-to-all-done.1 = bf16[128,4,4]{0,2,1:T(4,128)(2,1)S(1)} async-done(((bf16[128,4,4]{0,2,1:T(4,128)(2,1)}), bf16[128,4,4]{0,2,1:T(4,128)(2,1)S(1)}, u32[]{:S(2)}, u32[]{:S(2)}) %all-to-all-start.1) | async-done | bytes 4128 | tf_op jit(solution)/shard_map/all_to_all | solution.py:75
  20.1 3.5 %all-to-all-start.5 = ((bf16[128,4,256]{0,2,1:T(8,128)(2,1)}), bf16[128,4,256]{0,2,1:T(8,128)(2,1)S(1)}, u32[]{:S(2)}, u32[]{:S(2)}) async-start(bf16[128,4,256]{0,2,1:T(8,128)(2,1)} %bitcast.24), calls=%async_computation.5 | async-start | bytes 524288 | tf_op jit(solution)/shard_map/all_to_all | solution.py:71
  24.5 7.0 %all-to-all-done.5 = bf16[128,4,256]{0,2,1:T(8,128)(2,1)S(1)} async-done(((bf16[128,4,256]{0,2,1:T(8,128)(2,1)}), bf16[128,4,256]{0,2,1:T(8,128)(2,1)S(1)}, u32[]{:S(2)}, u32[]{:S(2)}) %all-to-all-start.5) | async-done | bytes 262176 | tf_op jit(solution)/shard_map/all_to_all | solution.py:71
  31.5 3.4 %all-to-all-start = ((bf16[128,4,256]{0,2,1:T(8,128)(2,1)}), bf16[128,4,256]{0,2,1:T(8,128)(2,1)S(1)}, u32[]{:S(2)}, u32[]{:S(2)}) async-start(bf16[128,4,256]{0,2,1:T(8,128)(2,1)} %bitcast), calls=%async_computation | async-start | bytes 524288 | tf_op jit(solution)/shard_map/all_to_all | solution.py:72
  36.6 12.5 %all_gather.3 = bf16[512,64]{0,1:T(8,128)(2,1)S(1)} all-gather(bf16[128,64]{0,1:T(8,128)(2,1)S(1)} %copy-done.31), channel_id=1, replica_groups=mesh['sp'=4,'dp'=8] {'sp'}, dimensions={0}, use_global_device_ids=true | all-gather | bytes 81920 | tf_op jit(solution)/shard_map/all_gather | solution.py:78
  51.7 4.1 %all-to-all-start.3 = ((bf16[128,4,512]{2,0,1:T(8,128)(2,1)}), bf16[128,4,512]{2,0,1:T(8,128)(2,1)}, u32[]{:S(2)}, u32[]{:S(2)}) async-start(bf16[128,4,512]{2,0,1:T(8,128)(2,1)} %bitcast.143), calls=%async_computation.3 | async-start | bytes 1048576 | tf_op jit(solution)/shard_map/all_to_all | solution.py:74
  58.0 25.9 %fusion.46 = f32[4,8,64,64]{3,1,2,0:T(8,128)S(1)} fusion(f32[4,8,64,64]{3,1,2,0:T(8,128)S(1)} %copy.194), kind=kOutput, calls=%fused_computation.93 | output fusion | flops 8257536 | bytes 1048576 | tf_op jit(solution)/shard_map/jvp(jit(cumsum))/reduce_window_sum | solution.py:34
  83.9 5.1 %all-to-all-start.2 = ((bf16[128,4,512]{2,0,1:T(8,128)(2,1)}), bf16[128,4,512]{2,0,1:T(8,128)(2,1)}, u32[]{:S(2)}, u32[]{:S(2)}) async-start(bf16[128,4,512]{2,0,1:T(8,128)(2,1)} %bitcast.144), calls=%async_computation.2 | async-start | bytes 1048576 | tf_op jit(solution)/shard_map/all_to_all | solution.py:73
  95.1 2.0 reshape.161
  97.0 1.9 copy.205
  99.3 2.0 reshape.159
  103.7 2.9 %convolution_bitcast_fusion = f32[8,4,64,128]{3,0,2,1:T(8,128)S(1)} fusion(f32[4,64,128,8]{2,1,3,0:T(8,128)S(1)} %convolution_bitcast_fusion.3, f32[4,8,64]{1,2,0:T(8,128)S(1)} %copy-done.23, f32[4,8,64]{1,2,0:T(8,128)S(1)} %copy-done.24, pred[8,8]{1,0:T(8,128)(4,1)S(1)} %copy-done.32), kind=kOutput, calls=%fused_computation.4 | convolution fusion | flops 25214976 | bytes 2113600 | tf_op jit(solution)/shard_map/transpose(jvp(hnmk,mhkv->nhkv))/dot_general | solution.py:23
  106.6 2.8 %fusion.18 = (f32[4,8,64]{2,1,0:T(8,128)}, f32[4,8,64,64]{2,3,1,0:T(8,128)S(1)}, f32[4,8,64,64]{2,3,1,0:T(8,128)}) fusion(f32[4,8,64,64]{2,3,1,0:T(8,128)S(1)} %copy.195, f32[4,8,64,64]{2,1,3,0:T(8,128)S(1)} %reshape.166, f32[4,8,64]{2,1,0:T(8,128)S(1)} %slice_bitcast_fusion, bf16[4,8,64,128]{3,2,1,0:T(8,128)(2,1)S(1)} %bitcast.150, ...), kind=kOutput, calls=%fused_computation.40 | convolution fusion | flops 201979904 | bytes 3686400 | tf_op jit(solution)/shard_map/transpose(jvp(hnjk,hnjv->nhkv))/dot_general | solution.py:46
  110.4 2.5 convolution_bitcast_fusion.1
  112.9 4.3 %fusion.45 = (f32[4,8,64]{1,2,0:T(8,128)}, f32[4,8,64]{1,2,0:T(8,128)}) fusion(f32[4,8,64]{1,2,0:T(8,128)S(1)} %copy-done.23, f32[4,8,64]{1,2,0:T(8,128)S(1)} %copy-done.24, f32[8,4,64,128]{3,2,1,0:T(8,128)S(1)} %fusion.6, f32[4,64,128,8]{2,1,3,0:T(8,128)S(1)} %convolution_bitcast_fusion.3, pred[8,8]{1,0:T(8,128)(4,1)S(1)} %copy-done.32), kind=kOutput, calls=%fused_computation.92 | convolution fusion | flops 25276416 | bytes 2129984 | tf_op jit(solution)/shard_map/transpose(jvp(hnmk,mhkv->nhkv))/dot_general | solution.py:23
  117.2 2.0 convolution_bitcast_fusion.4
  130.1 3.8 %pad_add_fusion = (f32[4,8,64,64]{2,3,1,0:T(8,128)}, bf16[4,8,64,64]{2,3,1,0:T(8,128)(2,1)}, bf16[4,8,64,64]{2,3,1,0:T(8,128)(2,1)}) fusion(f32[4,8,1,64]{2,3,1,0:T(8,128)S(1)} %fusion.3, f32[4,8,64,64]{2,3,1,0:T(8,128)S(1)} %fusion.44, f32[4,8,64,64]{2,1,3,0:T(8,128)S(1)} %mul.75, f32[4,8,64,64]{2,3,1,0:T(8,128)S(1)} %copy.195, ...), kind=kOutput, calls=%fused_computation.22 | convolution fusion | flops 103677952 | bytes 4734976 | tf_op jit(solution)/shard_map/transpose(jvp(hnik,hnjk->hnij))/dot_general | solution.py:41
  133.9 2.5 copy.246
  136.4 3.3 %fusion.47 = f32[4,8,64,64]{3,1,2,0:T(8,128)} fusion(f32[4,8,64,64]{3,1,2,0:T(8,128)} %copy.246), kind=kOutput, calls=%fused_computation.94 | output fusion | flops 8257536 | bytes 1048576 | tf_op jit(solution)/shard_map/transpose(jvp(jit(cumsum)))/reduce_window_sum | solution.py:34
  139.7 2.6 %copy.247 = f32[4,8,64,64]{2,1,3,0:T(8,128)} copy(f32[4,8,64,64]{3,1,2,0:T(8,128)} %fusion.47) | data formatting | bytes 1048576 | tf_op jit(solution)/shard_map/transpose(jvp(jit(cumsum)))/reduce_window_sum | solution.py:34
  142.2 2.3 reshape.163
  147.5 3.1 %convolution_select_fusion.2 = f32[4,8,64,64]{3,2,1,0:T(8,128)} fusion(pred[64,64]{1,0:T(8,128)(4,1)S(1)} %copy-done.28, f32[4,8,64,64]{2,1,3,0:T(8,128)S(1)} %reshape.166, f32[4,8,64,64]{2,3,1,0:T(8,128)S(1)} %copy.195, f32[4,8,64,64]{2,1,3,0:T(8,128)S(1)} %mul.75), kind=kOutput, calls=%fused_computation.11 | convolution fusion | flops 101187584 | bytes 2101248 | tf_op jit(solution)/shard_map/jvp(hnik,hnjk->hnij)/dot_general | solution.py:41
  152.1 4.7 %all-to-all-start.4 = ((bf16[4,128,256]{1,2,0:T(8,128)(2,1)}), bf16[4,128,256]{1,2,0:T(8,128)(2,1)}, u32[]{:S(2)}, u32[]{:S(2)}) async-start(bf16[4,128,256]{1,2,0:T(8,128)(2,1)} %copy.213), calls=%async_computation.4 | async-start | bytes 524288 | tf_op jit(solution)/shard_map/all_to_all | solution.py:101
  156.8 44.4 %all-reduce.3.cloned.1.call-done = f32[64,256]{1,0:T(8,128)} async-done(((f32[64,256]{1,0:T(8,128)}), f32[64,256]{1,0:T(8,128)}) %all-reduce.3.cloned.1.call-update) | async-done | bytes 65552 | tf_op jit(solution)/shard_map/psum | solution.py:122
  202.7 3.1 %fusion.11 = f32[4,8,64,128]{3,2,1,0:T(8,128)S(1)} fusion(f32[4,8,64,64]{2,3,1,0:T(8,128)S(1)} %copy-done.4, f32[8,4,64,128]{3,0,2,1:T(8,128)} %copy-done.8), kind=kOutput, calls=%fused_computation.30 | convolution fusion | flops 201326592 | bytes 2621440 | tf_op jit(solution)/shard_map/transpose(jvp(hnjk,hnjv->nhkv))/dot_general | solution.py:46
  210.1 3.8 %collective-permute-done.1 = f32[64,256]{1,0:T(8,128)} collective-permute-done((f32[64,256]{1,0:T(8,128)}, f32[64,256]{1,0:T(8,128)}, u32[]{:S(2)}, u32[]{:S(2)}) %collective-permute-start.1) | collective-permute-done | bytes 65568 | tf_op jit(solution)/shard_map/ppermute | solution.py:125
  214.0 5.1 %all-to-all-start.6 = ((bf16[4,128,256]{1,2,0:T(8,128)(2,1)}), bf16[4,128,256]{1,2,0:T(8,128)(2,1)S(1)}, u32[]{:S(2)}, u32[]{:S(2)}) async-start(bf16[4,128,256]{1,2,0:T(8,128)(2,1)} %copy.226), calls=%async_computation.6 | async-start | bytes 524288 | tf_op jit(solution)/shard_map/all_to_all | solution.py:104
  222.2 3.7 %all-to-all-done.6 = bf16[4,128,256]{1,2,0:T(8,128)(2,1)S(1)} async-done(((bf16[4,128,256]{1,2,0:T(8,128)(2,1)}), bf16[4,128,256]{1,2,0:T(8,128)(2,1)S(1)}, u32[]{:S(2)}, u32[]{:S(2)}) %all-to-all-start.6) | async-done | bytes 262176 | tf_op jit(solution)/shard_map/all_to_all | solution.py:104
  225.9 3.5 %all-to-all-start.7 = ((bf16[4,128,512]{2,1,0:T(8,128)(2,1)}), bf16[4,128,512]{2,1,0:T(8,128)(2,1)S(1)}, u32[]{:S(2)}, u32[]{:S(2)}) async-start(bf16[4,128,512]{2,1,0:T(8,128)(2,1)} %convert_element_type.84), calls=%async_computation.7 | async-start | bytes 1048576 | tf_op jit(solution)/shard_map/all_to_all | solution.py:107
  232.7 9.2 %reduce-scatter.2.cloned.1.call-done = f32[128,64]{0,1:T(8,128)} async-done(((f32[512,64]{0,1:T(8,128)}), f32[128,64]{0,1:T(8,128)}) %reduce-scatter.2.cloned.1.call-update) | async-done | bytes 32784 | tf_op jit(solution)/shard_map/reduce_scatter | solution.py:116
  243.2 1.8 copy.248
  (145 shorter events, 49.6 us)
Async XLA Ops:
  8.0 41.7 %copy-start = (bf16[64,1024]{1,0:T(8,128)(2,1)S(1)}, bf16[64,1024]{1,0:T(8,128)(2,1)}, u32[]{:S(2)}) copy-start(bf16[64,1024]{1,0:T(8,128)(2,1)} %param.13) | copy-start | bytes 393220
  8.0 12.1 %all-to-all-start.1 = ((bf16[128,4,4]{0,2,1:T(4,128)(2,1)}), bf16[128,4,4]{0,2,1:T(4,128)(2,1)S(1)}, u32[]{:S(2)}, u32[]{:S(2)}) async-start(bf16[128,4,4]{0,2,1:T(4,128)(2,1)} %bitcast.168), calls=%async_computation.1 | async-start | bytes 8192 | tf_op jit(solution)/shard_map/all_to_all | solution.py:75
  20.1 3.6 %copy-start.19 = (bf16[128,1024]{1,0:T(8,128)(2,1)S(1)}, bf16[128,1024]{1,0:T(8,128)(2,1)}, u32[]{:S(2)}) copy-start(bf16[128,1024]{1,0:T(8,128)(2,1)} %param.9) | copy-start | bytes 786436
  20.1 11.4 %all-to-all-start.5 = ((bf16[128,4,256]{0,2,1:T(8,128)(2,1)}), bf16[128,4,256]{0,2,1:T(8,128)(2,1)S(1)}, u32[]{:S(2)}, u32[]{:S(2)}) async-start(bf16[128,4,256]{0,2,1:T(8,128)(2,1)} %bitcast.24), calls=%async_computation.5 | async-start | bytes 524288 | tf_op jit(solution)/shard_map/all_to_all | solution.py:71
  23.6 11.3 %copy-start.17 = (bf16[128,2048]{1,0:T(8,128)(2,1)S(1)}, bf16[128,2048]{1,0:T(8,128)(2,1)}, u32[]{:S(2)}) copy-start(bf16[128,2048]{1,0:T(8,128)(2,1)} %param.11) | copy-start | bytes 1572868
  31.5 19.4 %all-to-all-start = ((bf16[128,4,256]{0,2,1:T(8,128)(2,1)}), bf16[128,4,256]{0,2,1:T(8,128)(2,1)S(1)}, u32[]{:S(2)}, u32[]{:S(2)}) async-start(bf16[128,4,256]{0,2,1:T(8,128)(2,1)} %bitcast), calls=%async_computation | async-start | bytes 524288 | tf_op jit(solution)/shard_map/all_to_all | solution.py:72
  35.0 1.6 copy-start.31
  49.1 1.9 copy-start.21
  51.0 5.4 %copy-start.18 = (bf16[128,2048]{1,0:T(8,128)(2,1)S(1)}, bf16[128,2048]{1,0:T(8,128)(2,1)}, u32[]{:S(2)}) copy-start(bf16[128,2048]{1,0:T(8,128)(2,1)} %param.10) | copy-start | bytes 1572868
  51.7 32.2 %all-to-all-start.3 = ((bf16[128,4,512]{2,0,1:T(8,128)(2,1)}), bf16[128,4,512]{2,0,1:T(8,128)(2,1)}, u32[]{:S(2)}, u32[]{:S(2)}) async-start(bf16[128,4,512]{2,0,1:T(8,128)(2,1)} %bitcast.143), calls=%async_computation.3 | async-start | bytes 1048576 | tf_op jit(solution)/shard_map/all_to_all | solution.py:74
  83.9 15.5 %all-to-all-start.2 = ((bf16[128,4,512]{2,0,1:T(8,128)(2,1)}), bf16[128,4,512]{2,0,1:T(8,128)(2,1)}, u32[]{:S(2)}, u32[]{:S(2)}) async-start(bf16[128,4,512]{2,0,1:T(8,128)(2,1)} %bitcast.144), calls=%async_computation.2 | async-start | bytes 1048576 | tf_op jit(solution)/shard_map/all_to_all | solution.py:73
  88.9 112.3 %all-reduce.3.cloned.1.call-start = ((), (), s32[]{:S(2)}) async-start(), calls=%async_computation.10 | async-start | bytes 131072 | tf_op jit(solution)/shard_map/psum | solution.py:122
  102.5 7.0 %copy-start.5 = (bf16[4,512,128]{2,1,0:T(8,128)(2,1)}, bf16[4,512,128]{2,1,0:T(8,128)(2,1)S(1)}, u32[]{:S(2)}) copy-start(bf16[4,512,128]{2,1,0:T(8,128)(2,1)S(1)} %copy.198) | copy-start | bytes 1572868
  106.6 2.9 %copy-start.8 = (f32[8,4,64,128]{3,0,2,1:T(8,128)}, f32[8,4,64,128]{3,0,2,1:T(8,128)S(1)}, u32[]{:S(2)}) copy-start(f32[8,4,64,128]{3,0,2,1:T(8,128)S(1)} %convolution_bitcast_fusion) | copy-start | bytes 3145732
  117.2 2.0 copy-start.26
  123.6 1.4 copy-start.27
  126.7 1.5 copy-start.11
  126.7 1.8 copy-start.12
  128.5 1.5 copy-start.7
  128.5 1.5 copy-start.9
  147.5 3.1 %copy-start.14 = (bf16[4,8,64,64]{2,3,1,0:T(8,128)(2,1)S(1)}, bf16[4,8,64,64]{2,3,1,0:T(8,128)(2,1)}, u32[]{:S(2)}) copy-start(bf16[4,8,64,64]{2,3,1,0:T(8,128)(2,1)} %get-tuple-element.26) | copy-start | bytes 786436
  150.9 51.8 %copy-start.4 = (f32[4,8,64,64]{2,3,1,0:T(8,128)S(1)}, f32[4,8,64,64]{2,3,1,0:T(8,128)}, u32[]{:S(2)}) copy-start(f32[4,8,64,64]{2,3,1,0:T(8,128)} %copy-done.3) | copy-start | bytes 1572868
  152.1 61.9 %all-to-all-start.4 = ((bf16[4,128,256]{1,2,0:T(8,128)(2,1)}), bf16[4,128,256]{1,2,0:T(8,128)(2,1)}, u32[]{:S(2)}, u32[]{:S(2)}) async-start(bf16[4,128,256]{1,2,0:T(8,128)(2,1)} %copy.213), calls=%async_computation.4 | async-start | bytes 524288 | tf_op jit(solution)/shard_map/all_to_all | solution.py:101
  156.8 50.8 %copy-start.2 = (bf16[4,512,128]{2,1,0:T(8,128)(2,1)S(1)}, bf16[4,512,128]{2,1,0:T(8,128)(2,1)}, u32[]{:S(2)}) copy-start(bf16[4,512,128]{2,1,0:T(8,128)(2,1)} %copy.205) | copy-start | bytes 1572868
  156.8 50.8 %copy-start.6 = (f32[4,8,64,64]{3,2,1,0:T(8,128)S(1)}, f32[4,8,64,64]{3,2,1,0:T(8,128)}, u32[]{:S(2)}) copy-start(f32[4,8,64,64]{3,2,1,0:T(8,128)} %convolution_select_fusion.2) | copy-start | bytes 1572868
  201.2 6.4 %collective-permute-start = (f32[64,256]{1,0:T(8,128)}, f32[64,256]{1,0:T(8,128)}, u32[]{:S(2)}, u32[]{:S(2)}) collective-permute-start(f32[64,256]{1,0:T(8,128)} %all-reduce.3.cloned.1.call-done), channel_id=1, source_target_pairs={{0,8},{8,16},{16,24},{24,0},{1,9},{9,17},{17,25},{25,1},{2,10},{10... | collective-permute-start | bytes 196616 | tf_op jit(solution)/shard_map/ppermute | solution.py:125
  205.8 2.8 %copy-start.13 = (bf16[4,8,64,64]{2,3,1,0:T(8,128)(2,1)S(1)}, bf16[4,8,64,64]{2,3,1,0:T(8,128)(2,1)}, u32[]{:S(2)}) copy-start(bf16[4,8,64,64]{2,3,1,0:T(8,128)(2,1)} %get-tuple-element.23) | copy-start | bytes 786436
  207.6 6.4 %collective-permute-start.1 = (f32[64,256]{1,0:T(8,128)}, f32[64,256]{1,0:T(8,128)}, u32[]{:S(2)}, u32[]{:S(2)}) collective-permute-start(f32[64,256]{1,0:T(8,128)} %collective-permute-done), channel_id=1, source_target_pairs={{0,8},{8,16},{16,24},{24,0},{1,9},{9,17},{17,25},{25,1},{2,10},{10... | collective-permute-start | bytes 196616 | tf_op jit(solution)/shard_map/ppermute | solution.py:125
  214.0 7.3 %collective-permute-start.2 = (f32[64,256]{1,0:T(8,128)}, f32[64,256]{1,0:T(8,128)S(1)}, u32[]{:S(2)}, u32[]{:S(2)}) collective-permute-start(f32[64,256]{1,0:T(8,128)} %collective-permute-done.1), channel_id=1, source_target_pairs={{0,8},{8,16},{16,24},{24,0},{1,9},{9,17},{17,25},{25,1},{2,10},{10... | collective-permute-start | bytes 196616 | tf_op jit(solution)/shard_map/ppermute | solution.py:125
  214.0 11.9 %all-to-all-start.6 = ((bf16[4,128,256]{1,2,0:T(8,128)(2,1)}), bf16[4,128,256]{1,2,0:T(8,128)(2,1)S(1)}, u32[]{:S(2)}, u32[]{:S(2)}) async-start(bf16[4,128,256]{1,2,0:T(8,128)(2,1)} %copy.226), calls=%async_computation.6 | async-start | bytes 524288 | tf_op jit(solution)/shard_map/all_to_all | solution.py:104
  219.1 22.8 %reduce-scatter.2.cloned.1.call-start = ((), (), s32[]{:S(2)}) async-start(), calls=%async_computation.9 | async-start | bytes 163840 | tf_op jit(solution)/shard_map/reduce_scatter | solution.py:116
  225.9 20.0 %all-to-all-start.7 = ((bf16[4,128,512]{2,1,0:T(8,128)(2,1)}), bf16[4,128,512]{2,1,0:T(8,128)(2,1)S(1)}, u32[]{:S(2)}, u32[]{:S(2)}) async-start(bf16[4,128,512]{2,1,0:T(8,128)(2,1)} %convert_element_type.84), calls=%async_computation.7 | async-start | bytes 1048576 | tf_op jit(solution)/shard_map/all_to_all | solution.py:107
  (14 other events, 14.5 us)
Sparse Core Ops, SparseCore 0:
  146.9 54.2 all-reduce.2
Sparse Core Ops, SparseCore 1:
  222.4 19.5 reduce-scatter.1
